TPU v7x, 512 devices: a whole 4x4x16 slice. The times are simulated.
512 devices in a mesh: fs: 16 (over y, x), tp: 32 (over z, core).
Axes of the slice: x: 4, y: 4, z: 16, core: 2. Of those that a mesh axis runs over, the one named last changes fastest.
Arguments:
- x_later: bfloat16 [6144, 2048], P('fs'), may hold values from -6 to 6
- x_earlier: bfloat16 [6144, 2048], P('fs'), may hold values from -6 to 6
- cot_hidden: bfloat16 [6144, 4096], P('fs', 'tp'), may hold values from -6 to 6
- w_gate: bfloat16 [2048, 4096], P('fs', 'tp'), may hold values from -0.125 to 0.125
- w_up: bfloat16 [2048, 4096], P('fs', 'tp'), may hold values from -0.125 to 0.125
- grad_gate: float32 [2048, 4096], P('fs', 'tp'), may hold values from -192 to 192
- grad_up: float32 [2048, 4096], P('fs', 'tp'), may hold values from -192 to 192
Outputs:
- hidden_later: bfloat16 [6144, 4096], P('fs', 'tp')
- grad_input: bfloat16 [6144, 2048], P('fs')
- new_grad_gate: float32 [2048, 4096], P('fs', 'tp')
- new_grad_up: float32 [2048, 4096], P('fs', 'tp')
All inputs are finite; a program needn't handle non-finite values.
Results may differ from a plain program's by a relative error of at most 0.018.
Values may be sent and summed in bfloat16 or wider, within the bound.
A program may use at most 64 MiB of HBM per device.

v0:
```python
import jax
import jax.numpy as jnp
from jax import lax
from jax.sharding import PartitionSpec as P


def contract_last(left, right):
    return lax.dot_general(
        left, right, (((1,), (1,)), ((), ())), preferred_element_type=jnp.float32
    )


def contract_first(left, right):
    return lax.dot_general(
        left, right, (((0,), (0,)), ((), ())), preferred_element_type=jnp.float32
    )


def per_device(x_later, x_earlier, cot_hidden, w_gate, w_up, grad_gate, grad_up):
    hidden_width = w_gate.shape[1]
    whole_gate, whole_up = (
        lax.all_gather(w_gate, "fs", axis=0, tiled=True),
        lax.all_gather(w_up, "fs", axis=0, tiled=True),
    )
    gate_later = jnp.dot(x_later, whole_gate, preferred_element_type=jnp.float32)
    up_later = jnp.dot(x_later, whole_up, preferred_element_type=jnp.float32)
    gate_earlier = jnp.dot(x_earlier, whole_gate, preferred_element_type=jnp.float32)
    up_earlier = jnp.dot(x_earlier, whole_up, preferred_element_type=jnp.float32)
    hidden_later = (jax.nn.silu(gate_later) * up_later).astype(jnp.bfloat16)
    sigma = jax.nn.sigmoid(gate_earlier)
    cotangent = cot_hidden.astype(jnp.float32)
    delta_up = (cotangent * gate_earlier * sigma).astype(jnp.bfloat16)
    delta_gate = (cotangent * up_earlier * sigma * (1.0 + gate_earlier * (1.0 - sigma))).astype(
        jnp.bfloat16
    )
    grad_share = lax.psum_scatter(
        (contract_last(delta_gate, whole_gate) + contract_last(delta_up, whole_up)).astype(
            jnp.bfloat16
        ),
        "tp",
        scatter_dimension=0,
        tiled=True,
    )
    grad_input = lax.all_gather(grad_share, "tp", axis=0, tiled=True)
    deltas = jnp.concatenate([delta_gate, delta_up], 1)
    summed = lax.psum_scatter(
        contract_first(x_earlier, deltas).astype(jnp.bfloat16),
        "fs",
        scatter_dimension=0,
        tiled=True,
    ).astype(jnp.float32)
    new_grad_gate = grad_gate + summed[:, :hidden_width]
    new_grad_up = grad_up + summed[:, hidden_width:]
    return (hidden_later, grad_input, new_grad_gate, new_grad_up)


def solution(mesh):
    placed = (
        P("fs", None),
        P("fs", None),
        P("fs", "tp"),
        P("fs", "tp"),
        P("fs", "tp"),
        P("fs", "tp"),
        P("fs", "tp"),
    )
    return jax.shard_map(
        per_device,
        mesh=mesh,
        in_specs=placed,
        out_specs=(P("fs", "tp"), P("fs", None), P("fs", "tp"), P("fs", "tp")),
        check_vma=False,
    )
```

profile of v0, /device:TPU:1, one launch (start us, length us, event | category | flops | bytes accessed | tf_op | source)
XLA Modules:
  0.0 242.5 jit_solution(5092972627354294884)
XLA Ops:
  8.0 0.0 reduce-scatter.6.cloned.1.call-start
  8.1 20.1 %all_gather.10 = bf16[2048,128]{1,0:T(8,128)(2,1)S(1)} all-gather(bf16[128,128]{1,0:T(8,128)(2,1)} %param.11), channel_id=1, replica_groups=mesh['fs'=16,'tp'=32] {'fs'}, dimensions={0}, use_global_device_ids=true | all-gather | bytes 557056 | tf_op jit(solution)/shard_map/all_gather | solution.py:23
  28.1 17.9 %all_gather.9 = bf16[2048,128]{1,0:T(8,128)(2,1)S(1)} all-gather(bf16[128,128]{1,0:T(8,128)(2,1)} %param.10), channel_id=1, replica_groups=mesh['fs'=16,'tp'=32] {'fs'}, dimensions={0}, use_global_device_ids=true | all-gather | bytes 557056 | tf_op jit(solution)/shard_map/all_gather | solution.py:22
  46.1 1.7 fusion.7
  47.8 0.6 fusion.5
  48.4 0.7 fusion.1
  49.1 1.3 copy.37
  50.4 0.0 all-gather.3.cloned.1.call-start
  50.5 0.6 fusion.13
  51.1 0.5 copy-done.4
  51.5 0.6 add_convert_fusion
  52.2 74.8 %fusion = bf16[16,2048]{1,0:T(8,128)(2,1)S(1)} fusion(bf16[384,2048]{1,0:T(8,128)(2,1)S(1)} %add_convert_fusion), kind=kCustom, calls=%all-reduce-scatter | all-reduce-scatter fusion | flops 1048577 | bytes 1640448
  127.0 3.4 %collective-permute-start.6 = (bf16[16,2048]{1,0:T(8,128)(2,1)S(1)}, bf16[16,2048]{1,0:T(8,128)(2,1)S(1)}, u32[]{:S(2)}, u32[]{:S(2)}) collective-permute-start(bf16[16,2048]{1,0:T(8,128)(2,1)S(1)} %fusion), channel_id=1, source_target_pairs={{0,7},{1,8},{2,9},{3,10},{4,11},{5,12},{6,13},{7,14},{8,15},{9,16}... | collective-permute-start | bytes 196616
  130.4 4.5 %collective-permute-start.5 = (bf16[16,2048]{1,0:T(8,128)(2,1)S(1)}, bf16[16,2048]{1,0:T(8,128)(2,1)S(1)}, u32[]{:S(2)}, u32[]{:S(2)}) collective-permute-start(bf16[16,2048]{1,0:T(8,128)(2,1)S(1)} %fusion), channel_id=1, source_target_pairs={{0,6},{1,7},{2,8},{3,9},{4,10},{5,11},{6,12},{7,13},{8,14},{9,15},... | collective-permute-start | bytes 196616
  134.9 6.2 %collective-permute-start.7 = (bf16[12,2048]{1,0:T(8,128)(2,1)S(1)}, bf16[12,2048]{1,0:T(8,128)(2,1)S(1)}, u32[]{:S(2)}, u32[]{:S(2)}) collective-permute-start(bf16[12,2048]{1,0:T(8,128)(2,1)S(1)} %slice.10), channel_id=1, source_target_pairs={{0,8},{1,9},{2,10},{3,11},{4,12},{5,13},{6,14},{7,15},{8,16},{9,17... | collective-permute-start | bytes 147464
  141.1 1.7 collective-permute-start.4
  142.8 6.4 %collective-permute-start.3 = (bf16[16,2048]{1,0:T(8,128)(2,1)S(1)}, bf16[16,2048]{1,0:T(8,128)(2,1)S(1)}, u32[]{:S(2)}, u32[]{:S(2)}) collective-permute-start(bf16[16,2048]{1,0:T(8,128)(2,1)S(1)} %fusion), channel_id=1, source_target_pairs={{0,4},{1,5},{2,6},{3,7},{4,8},{5,9},{6,10},{7,11},{8,12},{9,13},{1... | collective-permute-start | bytes 196616
  149.3 1.6 collective-permute-start.2
  150.9 2.8 %collective-permute-start.1 = (bf16[16,2048]{1,0:T(8,128)(2,1)S(1)}, bf16[16,2048]{1,0:T(8,128)(2,1)S(1)}, u32[]{:S(2)}, u32[]{:S(2)}) collective-permute-start(bf16[16,2048]{1,0:T(8,128)(2,1)S(1)} %fusion), channel_id=1, source_target_pairs={{0,2},{1,3},{2,4},{3,5},{4,6},{5,7},{6,8},{7,9},{8,10},{9,11},{10,... | collective-permute-start | bytes 196616
  153.7 2.2 collective-permute-start
  155.9 1.3 dynamic-slice.4
  157.9 1.5 concatenate.4
  159.4 0.7 dynamic-slice_bitcast_fusion
  160.1 0.1 copy.32
  160.2 0.1 copy.31
  160.3 2.1 fusion.12
  162.4 1.2 fusion.4
  163.6 0.9 copy.38
  164.6 0.7 copy.33
  165.4 0.7 copy.34
  166.1 65.4 %all-gather.3.cloned.1.call-done = bf16[32,12,2048]{2,1,0:T(8,128)(2,1)} async-done(((bf16[1,12,2048]{2,1,0:T(8,128)(2,1)}), bf16[32,12,2048]{2,1,0:T(8,128)(2,1)}) %all-gather.3.cloned.1.call-update) | async-done | bytes 1572880 | tf_op jit(solution)/shard_map/all_gather | solution.py:44
  231.4 3.6 %reshape.9 = bf16[384,2048]{1,0:T(8,128)(2,1)} reshape(bf16[32,12,2048]{2,1,0:T(8,128)(2,1)} %all-gather.3.cloned.1.call-done) | data formatting | bytes 3145728
  (33 shorter events, 0.2 us)
Async XLA Ops:
  8.0 38.1 %copy-start = (bf16[384,2048]{1,0:T(8,128)(2,1)S(1)}, bf16[384,2048]{1,0:T(8,128)(2,1)}, u32[]{:S(2)}) copy-start(bf16[384,2048]{1,0:T(8,128)(2,1)} %param.8) | copy-start | bytes 4718596
  8.0 155.6 %reduce-scatter.6.cloned.1.call-start = ((), (), s32[]{:S(2)}) async-start(), calls=%async_computation.2 | async-start | bytes 1114112
  28.1 19.6 %copy-start.3 = (bf16[2048,128]{1,0:T(8,128)(2,1)}, bf16[2048,128]{1,0:T(8,128)(2,1)S(1)}, u32[]{:S(2)}) copy-start(bf16[2048,128]{1,0:T(8,128)(2,1)S(1)} %all_gather.10) | copy-start | bytes 1572868
  46.1 4.4 %copy-start.1 = (bf16[2048,128]{1,0:T(8,128)(2,1)}, bf16[2048,128]{1,0:T(8,128)(2,1)S(1)}, u32[]{:S(2)}) copy-start(bf16[2048,128]{1,0:T(8,128)(2,1)S(1)} %all_gather.9) | copy-start | bytes 1572868
  46.1 1.7 copy-start.9
  50.4 181.0 %all-gather.3.cloned.1.call-start = ((), (), s32[]{:S(2)}) async-start(), calls=%async_computation.1 | async-start | bytes 2162688 | tf_op jit(solution)/shard_map/all_gather | solution.py:44
  50.5 1.0 copy-start.4
  52.1 107.9 %copy-start.7 = (f32[128,128]{1,0:T(8,128)S(1)}, f32[128,128]{1,0:T(8,128)}, u32[]{:S(2)}) copy-start(f32[128,128]{1,0:T(8,128)} %param.13) | copy-start | bytes 196612
  52.1 108.0 %copy-start.8 = (f32[128,128]{1,0:T(8,128)S(1)}, f32[128,128]{1,0:T(8,128)}, u32[]{:S(2)}) copy-start(f32[128,128]{1,0:T(8,128)} %param.12) | copy-start | bytes 196612
  127.0 33.3 %copy-start.2 = (bf16[2048,128]{1,0:T(8,128)(2,1)S(1)}, bf16[2048,128]{1,0:T(8,128)(2,1)}, u32[]{:S(2)}) copy-start(bf16[2048,128]{1,0:T(8,128)(2,1)} %copy-done.1) | copy-start | bytes 1572868
  127.0 24.0 %collective-permute-start.6 = (bf16[16,2048]{1,0:T(8,128)(2,1)S(1)}, bf16[16,2048]{1,0:T(8,128)(2,1)S(1)}, u32[]{:S(2)}, u32[]{:S(2)}) collective-permute-start(bf16[16,2048]{1,0:T(8,128)(2,1)S(1)} %fusion), channel_id=1, source_target_pairs={{0,7},{1,8},{2,9},{3,10},{4,11},{5,12},{6,13},{7,14},{8,15},{9,16}... | collective-permute-start | bytes 196616
  130.4 23.3 %collective-permute-start.5 = (bf16[16,2048]{1,0:T(8,128)(2,1)S(1)}, bf16[16,2048]{1,0:T(8,128)(2,1)S(1)}, u32[]{:S(2)}, u32[]{:S(2)}) collective-permute-start(bf16[16,2048]{1,0:T(8,128)(2,1)S(1)} %fusion), channel_id=1, source_target_pairs={{0,6},{1,7},{2,8},{3,9},{4,10},{5,11},{6,12},{7,13},{8,14},{9,15},... | collective-permute-start | bytes 196616
  134.9 14.4 %collective-permute-start.7 = (bf16[12,2048]{1,0:T(8,128)(2,1)S(1)}, bf16[12,2048]{1,0:T(8,128)(2,1)S(1)}, u32[]{:S(2)}, u32[]{:S(2)}) collective-permute-start(bf16[12,2048]{1,0:T(8,128)(2,1)S(1)} %slice.10), channel_id=1, source_target_pairs={{0,8},{1,9},{2,10},{3,11},{4,12},{5,13},{6,14},{7,15},{8,16},{9,17... | collective-permute-start | bytes 147464
  141.1 16.7 %collective-permute-start.4 = (bf16[16,2048]{1,0:T(8,128)(2,1)S(1)}, bf16[16,2048]{1,0:T(8,128)(2,1)S(1)}, u32[]{:S(2)}, u32[]{:S(2)}) collective-permute-start(bf16[16,2048]{1,0:T(8,128)(2,1)S(1)} %fusion), channel_id=1, source_target_pairs={{0,5},{1,6},{2,7},{3,8},{4,9},{5,10},{6,11},{7,12},{8,13},{9,14},{... | collective-permute-start | bytes 196616
  142.8 15.0 %collective-permute-start.3 = (bf16[16,2048]{1,0:T(8,128)(2,1)S(1)}, bf16[16,2048]{1,0:T(8,128)(2,1)S(1)}, u32[]{:S(2)}, u32[]{:S(2)}) collective-permute-start(bf16[16,2048]{1,0:T(8,128)(2,1)S(1)} %fusion), channel_id=1, source_target_pairs={{0,4},{1,5},{2,6},{3,7},{4,8},{5,9},{6,10},{7,11},{8,12},{9,13},{1... | collective-permute-start | bytes 196616
  149.3 8.6 %collective-permute-start.2 = (bf16[16,2048]{1,0:T(8,128)(2,1)S(1)}, bf16[16,2048]{1,0:T(8,128)(2,1)S(1)}, u32[]{:S(2)}, u32[]{:S(2)}) collective-permute-start(bf16[16,2048]{1,0:T(8,128)(2,1)S(1)} %fusion), channel_id=1, source_target_pairs={{0,3},{1,4},{2,5},{3,6},{4,7},{5,8},{6,9},{7,10},{8,11},{9,12},{10... | collective-permute-start | bytes 196616
  150.9 6.9 %collective-permute-start.1 = (bf16[16,2048]{1,0:T(8,128)(2,1)S(1)}, bf16[16,2048]{1,0:T(8,128)(2,1)S(1)}, u32[]{:S(2)}, u32[]{:S(2)}) collective-permute-start(bf16[16,2048]{1,0:T(8,128)(2,1)S(1)} %fusion), channel_id=1, source_target_pairs={{0,2},{1,3},{2,4},{3,5},{4,6},{5,7},{6,8},{7,9},{8,10},{9,11},{10,... | collective-permute-start | bytes 196616
  153.7 4.2 %collective-permute-start = (bf16[16,2048]{1,0:T(8,128)(2,1)S(1)}, bf16[16,2048]{1,0:T(8,128)(2,1)S(1)}, u32[]{:S(2)}, u32[]{:S(2)}) collective-permute-start(bf16[16,2048]{1,0:T(8,128)(2,1)S(1)} %fusion), channel_id=1, source_target_pairs={{0,1},{1,2},{2,3},{3,4},{4,5},{5,6},{6,7},{7,8},{8,9},{9,10},{10,1... | collective-permute-start | bytes 196616
  159.4 3.0 %copy-start.5 = (bf16[2048,128]{1,0:T(8,128)(2,1)S(1)}, bf16[2048,128]{1,0:T(8,128)(2,1)}, u32[]{:S(2)}) copy-start(bf16[2048,128]{1,0:T(8,128)(2,1)} %copy-done.3) | copy-start | bytes 1572868
  160.3 2.1 copy-start.6
Sparse Core Ops, SparseCore 0:
  50.6 100.0 reduce-scatter.5
Sparse Core Ops, SparseCore 1:
  160.1 71.2 all-gather.2
where the time goes:
time: 243 us; the launch traced here: 242 us
  blocking collectives  113 us (47%)
  waiting for transfers between devices  65.4 us (27%)
  starting transfers between devices  28.9 us (12%)
  between operations  16.5 us (7%)
  local copies, waits for them, and re-layouts  11.4 us (5%)
  matrix products  7.43 us (3%)
    unnamed x1, blocking collectives  74.8 us
    all_gather x1, waiting for transfers between devices, per_device(): grad_input = lax.all_gather(grad_share, 'tp', axis=0, tiled=True)  65.4 us
    unnamed x9, starting transfers between devices  28.9 us
    all_gather x1, blocking collectives, per_device(): lax.all_gather(w_up, 'fs', axis=0, tiled=True)  20.1 us
    all_gather x1, blocking collectives, per_device(): lax.all_gather(w_gate, 'fs', axis=0, tiled=True)  17.9 us
    unnamed x31, local copies, waits for them, and re-layouts  11.4 us
  transfers between devices with their start and end apart: 10, of which 1 were waited for; matrix products, arithmetic and copies ran while one was open for 35% of the time, Pallas kernels for 0%

commit v1 on v0

--- a/solution.py
+++ b/solution.py
@@ -41,7 +41,8 @@
         scatter_dimension=0,
         tiled=True,
     )
-    grad_input = lax.all_gather(grad_share, "tp", axis=0, tiled=True)
+    copies = jnp.concatenate([grad_share] * lax.axis_size("tp"), axis=0)
+    grad_input = lax.all_to_all(copies, "tp", 0, 0, tiled=True)
     deltas = jnp.concatenate([delta_gate, delta_up], 1)
     summed = lax.psum_scatter(
         contract_first(x_earlier, deltas).astype(jnp.bfloat16),

time: 243 us -> 283 us (1.16)
  waiting for transfers between devices: 65.4 us -> 90.2 us
  starting transfers between devices: 28.9 us -> 42 us
  local copies, waits for them, and re-layouts: 11.4 us -> 15.4 us
    unnamed x11 -> x10, waiting for transfers between devices: 0.06 us -> 85.6 us
    all_gather x1 -> x0, waiting for transfers between devices: 65.4 us -> none  [per_device(): grad_input = lax.all_gather(grad_share, 'tp', axis=0, tiled=True)]
    all_to_all x0 -> x1, starting transfers between devices: none -> 12.2 us  [per_device(): grad_input = lax.all_to_all(copies, 'tp', 0, 0, tiled=True)]
    all_to_all x0 -> x2, local copies, waits for them, and re-layouts: none -> 5.12 us  [per_device(): grad_input = lax.all_to_all(copies, 'tp', 0, 0, tiled=True)]
    unnamed x31 -> x28, local copies, waits for them, and re-layouts: 11.4 us -> 6.72 us
    all_to_all x0 -> x1, waiting for transfers between devices: none -> 4.59 us  [per_device(): grad_input = lax.all_to_all(copies, 'tp', 0, 0, tiled=True)]
    concatenate x0 -> x1, local copies, waits for them, and re-layouts: none -> 3.6 us  [per_device(): copies = jnp.concatenate([grad_share] * lax.axis_size('tp'), axis=0)]
  transfers between devices with their start and end apart: 10 -> 10, of which waited for: 1 -> 2; matrix products, arithmetic and copies ran while one was open for 35% -> 3% of each run, Pallas kernels for 0% -> 0%
where the time goes in v1:
time: 283 us; the launch traced here: 282 us
  blocking collectives  112 us (40%)
  waiting for transfers between devices  90.2 us (32%)
  starting transfers between devices  42 us (15%)
  local copies, waits for them, and re-layouts  15.4 us (5%)
  between operations  15.1 us (5%)
  matrix products  7.44 us (3%)
    unnamed x10, waiting for transfers between devices  85.6 us
    unnamed x1, blocking collectives  73.7 us
    unnamed x9, starting transfers between devices  29.7 us
    all_gather x1, blocking collectives, per_device(): lax.all_gather(w_up, 'fs', axis=0, tiled=True)  20.1 us
    all_gather x1, blocking collectives, per_device(): lax.all_gather(w_gate, 'fs', axis=0, tiled=True)  17.9 us
    all_to_all x1, starting transfers between devices, per_device(): grad_input = lax.all_to_all(copies, 'tp', 0, 0, tiled=True)  12.2 us
    unnamed x28, local copies, waits for them, and re-layouts  6.72 us
  transfers between devices with their start and end apart: 10, of which 2 were waited for; matrix products, arithmetic and copies ran while one was open for 3% of the time, Pallas kernels for 0%

profile of v1, /device:TPU:1, one launch (start us, length us, event | category | flops | bytes accessed | tf_op | source)
XLA Modules:
  0.0 281.8 jit_solution(18001259333146951667)
XLA Ops:
  7.2 20.1 %all_gather.7 = bf16[2048,128]{1,0:T(8,128)(2,1)S(1)} all-gather(bf16[128,128]{1,0:T(8,128)(2,1)} %param.11), channel_id=1, replica_groups=mesh['fs'=16,'tp'=32] {'fs'}, dimensions={0}, use_global_device_ids=true | all-gather | bytes 557056 | tf_op jit(solution)/shard_map/all_gather | solution.py:23
  27.3 17.9 %all_gather.6 = bf16[2048,128]{1,0:T(8,128)(2,1)S(1)} all-gather(bf16[128,128]{1,0:T(8,128)(2,1)} %param.10), channel_id=1, replica_groups=mesh['fs'=16,'tp'=32] {'fs'}, dimensions={0}, use_global_device_ids=true | all-gather | bytes 557056 | tf_op jit(solution)/shard_map/all_gather | solution.py:22
  45.2 1.7 fusion.7
  46.9 0.6 fusion.5
  47.5 0.6 fusion.13
  48.1 0.6 add_convert_fusion
  48.7 73.7 %fusion = bf16[16,2048]{1,0:T(8,128)(2,1)S(1)} fusion(bf16[384,2048]{1,0:T(8,128)(2,1)S(1)} %add_convert_fusion), kind=kCustom, calls=%all-reduce-scatter | all-reduce-scatter fusion | flops 1048577 | bytes 1640448
  122.4 3.6 %collective-permute-start.6 = (bf16[16,2048]{1,0:T(8,128)(2,1)S(1)}, bf16[16,2048]{1,0:T(8,128)(2,1)S(1)}, u32[]{:S(2)}, u32[]{:S(2)}) collective-permute-start(bf16[16,2048]{1,0:T(8,128)(2,1)S(1)} %fusion), channel_id=1, source_target_pairs={{0,7},{1,8},{2,9},{3,10},{4,11},{5,12},{6,13},{7,14},{8,15},{9,16}... | collective-permute-start | bytes 196616
  126.0 4.3 %collective-permute-start.5 = (bf16[16,2048]{1,0:T(8,128)(2,1)S(1)}, bf16[16,2048]{1,0:T(8,128)(2,1)S(1)}, u32[]{:S(2)}, u32[]{:S(2)}) collective-permute-start(bf16[16,2048]{1,0:T(8,128)(2,1)S(1)} %fusion), channel_id=1, source_target_pairs={{0,6},{1,7},{2,8},{3,9},{4,10},{5,11},{6,12},{7,13},{8,14},{9,15},... | collective-permute-start | bytes 196616
  130.3 6.6 %collective-permute-start.7 = (bf16[12,2048]{1,0:T(8,128)(2,1)S(1)}, bf16[12,2048]{1,0:T(8,128)(2,1)S(1)}, u32[]{:S(2)}, u32[]{:S(2)}) collective-permute-start(bf16[12,2048]{1,0:T(8,128)(2,1)S(1)} %slice.10), channel_id=1, source_target_pairs={{0,8},{1,9},{2,10},{3,11},{4,12},{5,13},{6,14},{7,15},{8,16},{9,17... | collective-permute-start | bytes 147464
  136.9 1.3 collective-permute-start.4
  138.2 7.4 %collective-permute-start.3 = (bf16[16,2048]{1,0:T(8,128)(2,1)S(1)}, bf16[16,2048]{1,0:T(8,128)(2,1)S(1)}, u32[]{:S(2)}, u32[]{:S(2)}) collective-permute-start(bf16[16,2048]{1,0:T(8,128)(2,1)S(1)} %fusion), channel_id=1, source_target_pairs={{0,4},{1,5},{2,6},{3,7},{4,8},{5,9},{6,10},{7,11},{8,12},{9,13},{1... | collective-permute-start | bytes 196616
  145.5 1.6 collective-permute-start.2
  147.2 2.8 collective-permute-start.1
  150.0 2.2 collective-permute-start
  152.2 1.3 dynamic-slice.4
  154.1 1.5 concatenate.8
  155.6 3.6 %concatenate.6 = bf16[384,2048]{1,0:T(8,128)(2,1)S(1)} concatenate(bf16[12,2048]{1,0:T(8,128)(2,1)S(1)} %constant_dynamic-slice_fusion, bf16[12,2048]{1,0:T(8,128)(2,1)S(1)} %constant_dynamic-slice_fusion, bf16[12,2048]{1,0:T(8,128)(2,1)S(1)} %constant_dynamic-slice_fusion, bf16[12,2048]{1,0:T(8,128)(2,1)S(1)} %constant_dynamic-slice_fusion, ...), dimensions={0} | concatenate | bytes 3145728 | tf_op jit(solution)/shard_map/concatenate | solution.py:44
  159.3 1.5 all_to_all.8
  160.8 12.2 %all-to-all-start = ((bf16[32,12,2048]{2,1,0:T(8,128)(2,1)}), bf16[32,12,2048]{2,1,0:T(8,128)(2,1)}, u32[]{:S(2)}, u32[]{:S(2)}) async-start(bf16[32,12,2048]{2,1,0:T(8,128)(2,1)} %all_to_all.8), calls=%async_computation | async-start | bytes 4194304 | tf_op jit(solution)/shard_map/all_to_all | solution.py:45
  173.1 0.7 fusion.1
  173.8 1.3 copy.37
  175.2 0.1 copy.32
  175.3 0.1 copy.31
  175.4 2.1 fusion.12
  177.5 1.2 fusion.4
  178.7 85.6 %reduce-scatter.6.cloned.1.call-done = bf16[128,256]{1,0:T(8,128)(2,1)} async-done(((bf16[2048,256]{1,0:T(8,128)(2,1)}), bf16[128,256]{1,0:T(8,128)(2,1)}) %reduce-scatter.6.cloned.1.call-update) | async-done | bytes 65552
  264.3 0.9 copy.38
  265.3 0.7 copy.33
  266.0 0.7 copy.34
  266.8 4.6 %all-to-all-done = bf16[32,12,2048]{2,1,0:T(8,128)(2,1)} async-done(((bf16[32,12,2048]{2,1,0:T(8,128)(2,1)}), bf16[32,12,2048]{2,1,0:T(8,128)(2,1)}, u32[]{:S(2)}, u32[]{:S(2)}) %all-to-all-start) | async-done | bytes 1572896 | tf_op jit(solution)/shard_map/all_to_all | solution.py:45
  271.4 3.6 %all_to_all.10 = bf16[384,2048]{1,0:T(8,128)(2,1)} reshape(bf16[32,12,2048]{2,1,0:T(8,128)(2,1)} %all-to-all-done) | data formatting | bytes 3145728 | tf_op jit(solution)/shard_map/all_to_all | solution.py:45
  (32 shorter events, 0.2 us)
Async XLA Ops:
  7.2 38.0 %copy-start = (bf16[384,2048]{1,0:T(8,128)(2,1)S(1)}, bf16[384,2048]{1,0:T(8,128)(2,1)}, u32[]{:S(2)}) copy-start(bf16[384,2048]{1,0:T(8,128)(2,1)} %param.8) | copy-start | bytes 4718596
  27.3 20.8 %copy-start.3 = (bf16[2048,128]{1,0:T(8,128)(2,1)}, bf16[2048,128]{1,0:T(8,128)(2,1)S(1)}, u32[]{:S(2)}) copy-start(bf16[2048,128]{1,0:T(8,128)(2,1)S(1)} %all_gather.7) | copy-start | bytes 1572868
  45.2 2.3 copy-start.1
  45.2 1.7 copy-start.8
  122.4 24.8 %collective-permute-start.6 = (bf16[16,2048]{1,0:T(8,128)(2,1)S(1)}, bf16[16,2048]{1,0:T(8,128)(2,1)S(1)}, u32[]{:S(2)}, u32[]{:S(2)}) collective-permute-start(bf16[16,2048]{1,0:T(8,128)(2,1)S(1)} %fusion), channel_id=1, source_target_pairs={{0,7},{1,8},{2,9},{3,10},{4,11},{5,12},{6,13},{7,14},{8,15},{9,16}... | collective-permute-start | bytes 196616
  126.0 24.0 %collective-permute-start.5 = (bf16[16,2048]{1,0:T(8,128)(2,1)S(1)}, bf16[16,2048]{1,0:T(8,128)(2,1)S(1)}, u32[]{:S(2)}, u32[]{:S(2)}) collective-permute-start(bf16[16,2048]{1,0:T(8,128)(2,1)S(1)} %fusion), channel_id=1, source_target_pairs={{0,6},{1,7},{2,8},{3,9},{4,10},{5,11},{6,12},{7,13},{8,14},{9,15},... | collective-permute-start | bytes 196616
  130.3 15.3 %collective-permute-start.7 = (bf16[12,2048]{1,0:T(8,128)(2,1)S(1)}, bf16[12,2048]{1,0:T(8,128)(2,1)S(1)}, u32[]{:S(2)}, u32[]{:S(2)}) collective-permute-start(bf16[12,2048]{1,0:T(8,128)(2,1)S(1)} %slice.10), channel_id=1, source_target_pairs={{0,8},{1,9},{2,10},{3,11},{4,12},{5,13},{6,14},{7,15},{8,16},{9,17... | collective-permute-start | bytes 147464
  136.9 17.2 %collective-permute-start.4 = (bf16[16,2048]{1,0:T(8,128)(2,1)S(1)}, bf16[16,2048]{1,0:T(8,128)(2,1)S(1)}, u32[]{:S(2)}, u32[]{:S(2)}) collective-permute-start(bf16[16,2048]{1,0:T(8,128)(2,1)S(1)} %fusion), channel_id=1, source_target_pairs={{0,5},{1,6},{2,7},{3,8},{4,9},{5,10},{6,11},{7,12},{8,13},{9,14},{... | collective-permute-start | bytes 196616
  138.2 15.9 %collective-permute-start.3 = (bf16[16,2048]{1,0:T(8,128)(2,1)S(1)}, bf16[16,2048]{1,0:T(8,128)(2,1)S(1)}, u32[]{:S(2)}, u32[]{:S(2)}) collective-permute-start(bf16[16,2048]{1,0:T(8,128)(2,1)S(1)} %fusion), channel_id=1, source_target_pairs={{0,4},{1,5},{2,6},{3,7},{4,8},{5,9},{6,10},{7,11},{8,12},{9,13},{1... | collective-permute-start | bytes 196616
  145.5 8.6 %collective-permute-start.2 = (bf16[16,2048]{1,0:T(8,128)(2,1)S(1)}, bf16[16,2048]{1,0:T(8,128)(2,1)S(1)}, u32[]{:S(2)}, u32[]{:S(2)}) collective-permute-start(bf16[16,2048]{1,0:T(8,128)(2,1)S(1)} %fusion), channel_id=1, source_target_pairs={{0,3},{1,4},{2,5},{3,6},{4,7},{5,8},{6,9},{7,10},{8,11},{9,12},{10... | collective-permute-start | bytes 196616
  147.2 6.9 %collective-permute-start.1 = (bf16[16,2048]{1,0:T(8,128)(2,1)S(1)}, bf16[16,2048]{1,0:T(8,128)(2,1)S(1)}, u32[]{:S(2)}, u32[]{:S(2)}) collective-permute-start(bf16[16,2048]{1,0:T(8,128)(2,1)S(1)} %fusion), channel_id=1, source_target_pairs={{0,2},{1,3},{2,4},{3,5},{4,6},{5,7},{6,8},{7,9},{8,10},{9,11},{10,... | collective-permute-start | bytes 196616
  150.0 4.2 %collective-permute-start = (bf16[16,2048]{1,0:T(8,128)(2,1)S(1)}, bf16[16,2048]{1,0:T(8,128)(2,1)S(1)}, u32[]{:S(2)}, u32[]{:S(2)}) collective-permute-start(bf16[16,2048]{1,0:T(8,128)(2,1)S(1)} %fusion), channel_id=1, source_target_pairs={{0,1},{1,2},{2,3},{3,4},{4,5},{5,6},{6,7},{7,8},{8,9},{9,10},{10,1... | collective-permute-start | bytes 196616
  160.8 110.6 %all-to-all-start = ((bf16[32,12,2048]{2,1,0:T(8,128)(2,1)}), bf16[32,12,2048]{2,1,0:T(8,128)(2,1)}, u32[]{:S(2)}, u32[]{:S(2)}) async-start(bf16[32,12,2048]{2,1,0:T(8,128)(2,1)} %all_to_all.8), calls=%async_computation | async-start | bytes 4194304 | tf_op jit(solution)/shard_map/all_to_all | solution.py:45
  173.0 91.3 %reduce-scatter.6.cloned.1.call-start = ((), (), s32[]{:S(2)}) async-start(), calls=%async_computation.2 | async-start | bytes 1114112
  173.8 1.4 copy-start.6
  173.8 1.5 copy-start.7
  173.8 1.6 copy-start.2
  175.1 2.4 copy-start.4
  175.4 2.1 copy-start.5
Sparse Core Ops, SparseCore 0:
  178.5 85.7 reduce-scatter.5
